TPU v7x, 32 devices: a whole 2x2x4 slice. The times are simulated.
32 devices in a mesh: rep: 2 (over x), fs: 8 (over z, y), tp: 2 (over core).
Axes of the slice: x: 2, y: 2, z: 4, core: 2. Of those that a mesh axis runs over, the one named last changes fastest.
Arguments:
- states: bfloat16 [6144, 2048], P(('rep', 'fs'), 'tp'), may hold values from -6 to 6
- mix_gain: float32 [2048], replicated, may hold values from 0.1 to 1.9
- w_value: bfloat16 [2048, 2048], P('fs', 'tp'), may hold values from -1 to 1
- w_gate: bfloat16 [2048, 2048], P('fs', 'tp'), may hold values from -0.125 to 0.125
- conv_kernel: float32 [31, 2048], replicated, may hold values from -1 to 1
- chan_gain: float32 [2048], replicated, may hold values from 0.1 to 1.9
- w_mix_out: bfloat16 [2048, 2048], P('fs', 'tp'), may hold values from -0.125 to 0.125
- mlp_gain: float32 [2048], replicated, may hold values from 0.1 to 1.9
- w_up: bfloat16 [2048, 6144], P('fs', 'tp'), may hold values from -0.125 to 0.125
- w_down_t: bfloat16 [2048, 6144], P('fs', 'tp'), may hold values from -0.078125 to 0.078125
Outputs:
- layer_out: bfloat16 [6144, 2048], P(('rep', 'fs'), 'tp')
All inputs are finite; a program needn't handle non-finite values.
Results may differ from a plain program's by a relative error of at most 0.017.
Values may be sent and summed in bfloat16 or wider, within the bound.
A program may use at most 64 MiB of HBM per device.

v0:
```python
import jax
import jax.numpy as jnp
from jax import lax
from jax.sharding import PartitionSpec as P

D = 2048
KWIDTH = 31
LENGTH = 128
EPS = 1e-06


def rms_norm(rows, gain):
    values = rows.astype(jnp.float32)
    scaled = values * lax.rsqrt(jnp.mean(values * values, axis=-1, keepdims=True) + EPS)
    return (scaled * gain).astype(jnp.bfloat16)


def times_transposed(left, right):
    return lax.dot_general(
        left, right, (((1,), (1,)), ((), ())), preferred_element_type=jnp.float32
    )


def body(
    states, mix_gain, w_value, w_gate, conv_kernel, chan_gain, w_mix_out, mlp_gain, w_up, w_down_t
):
    width = states.shape[1]
    offset = lax.axis_index("tp") * width
    token_rows = states.shape[0]
    whole_rows = lax.all_gather(states, "tp", axis=1, tiled=True)
    normed = rms_norm(whole_rows, mix_gain)
    columns = normed
    value = jnp.dot(
        columns,
        lax.all_gather(w_value, "fs", axis=0, tiled=True),
        preferred_element_type=jnp.float32,
    )
    gate = jnp.dot(
        columns,
        lax.all_gather(w_gate, "fs", axis=0, tiled=True),
        preferred_element_type=jnp.float32,
    )
    gated = value * jax.nn.sigmoid(gate)
    own_kernel = lax.dynamic_slice_in_dim(conv_kernel, offset, width, 1)
    blocks = gated.reshape(token_rows // LENGTH, LENGTH, width)
    padded = jnp.pad(blocks, ((0, 0), (KWIDTH - 1, 0), (0, 0)))
    filtered = jnp.zeros_like(blocks)
    for tap in range(KWIDTH):
        filtered = filtered + own_kernel[tap][None, None, :] * padded[:, tap : tap + LENGTH, :]
    filtered = filtered.reshape(token_rows, width)
    sum_rows, square_rows = lax.psum(
        (jnp.sum(filtered, axis=-1), jnp.sum(filtered * filtered, axis=-1)), "tp"
    )
    mean_rows = (sum_rows / D)[:, None]
    variance = (square_rows / D)[:, None] - mean_rows * mean_rows
    own_gain = lax.dynamic_slice_in_dim(chan_gain, offset, width, 0)
    activated = jax.nn.silu((filtered - mean_rows) * lax.rsqrt(variance + EPS) * own_gain).astype(
        jnp.bfloat16
    )
    mixer_terms = times_transposed(activated, lax.all_gather(w_mix_out, "fs", axis=0, tiled=True))
    mixed = lax.psum_scatter(
        mixer_terms.astype(jnp.bfloat16), "tp", scatter_dimension=1, tiled=True
    ).astype(jnp.float32)
    middle = (states.astype(jnp.float32) + mixed).astype(jnp.bfloat16)
    middle_rows = lax.all_gather(middle, "tp", axis=1, tiled=True)
    normed_mid = rms_norm(middle_rows, mlp_gain)
    columns = normed_mid
    upward = jnp.dot(
        columns, lax.all_gather(w_up, "fs", axis=0, tiled=True), preferred_element_type=jnp.float32
    )
    hidden = jnp.square(jnp.maximum(upward, 0.0)).astype(jnp.bfloat16)
    fed_terms = times_transposed(hidden, lax.all_gather(w_down_t, "fs", axis=0, tiled=True))
    fed = lax.psum_scatter(
        fed_terms.astype(jnp.bfloat16), "tp", scatter_dimension=1, tiled=True
    ).astype(jnp.float32)
    return (middle.astype(jnp.float32) + fed).astype(jnp.bfloat16)


def solution(mesh):
    in_specs = (
        P(("rep", "fs"), "tp"),
        P(),
        P("fs", "tp"),
        P("fs", "tp"),
        P(),
        P(),
        P("fs", "tp"),
        P(),
        P("fs", "tp"),
        P("fs", "tp"),
    )
    out_specs = P(("rep", "fs"), "tp")
    return jax.shard_map(body, mesh=mesh, in_specs=in_specs, out_specs=out_specs, check_vma=False)
```

profile of v0, /device:TPU:0, one launch (start us, length us, event | category | flops | bytes accessed | tf_op | source)
XLA Modules:
  0.0 658.4 jit_solution(12516439432388913050)
XLA Ops:
  6.5 0.7 all-gather.8.cloned.1.call-update
  7.3 0.7 all-gather.12.cloned.1.call-update
  8.1 0.7 all-gather.10.cloned.1.call-update
  8.8 0.5 all-gather.14.cloned.1.call-update
  9.3 0.0 reduce-scatter.3.cloned.1.call-start
  9.4 1.3 fusion.79
  10.7 1.5 constant_dynamic-slice_fusion
  12.2 9.2 %all-gather.8.cloned.1.call-done = bf16[384,2048]{1,0:T(8,128)(2,1)} async-done(((bf16[384,1024]{1,0:T(8,128)(2,1)}), bf16[384,2048]{1,0:T(8,128)(2,1)}) %all-gather.8.cloned.1.call-update) | async-done | bytes 1572880 | tf_op jit(solution)/shard_map/all_gather | solution.py:30
  21.4 1.9 fusion
  23.4 74.2 %all-gather.12.cloned.1.call-done = bf16[2048,1024]{1,0:T(8,128)(2,1)} async-done(((bf16[256,1024]{1,0:T(8,128)(2,1)}), bf16[2048,1024]{1,0:T(8,128)(2,1)}) %all-gather.12.cloned.1.call-update) | async-done | bytes 4194320 | tf_op jit(solution)/shard_map/all_gather | solution.py:40
  97.6 4.0 fusion.73
  101.6 69.5 %all-gather.10.cloned.1.call-done = bf16[2048,1024]{1,0:T(8,128)(2,1)} async-done(((bf16[256,1024]{1,0:T(8,128)(2,1)}), bf16[2048,1024]{1,0:T(8,128)(2,1)}) %all-gather.10.cloned.1.call-update) | async-done | bytes 4194320 | tf_op jit(solution)/shard_map/all_gather | solution.py:35
  171.0 4.1 divide_multiply_fusion
  175.2 7.0 %fusion.77 = (f32[3,128]{1,0:T(4,128)S(1)}, f32[3,128]{1,0:T(4,128)S(1)}, f32[3,128,1024]{2,1,0:T(8,128)S(1)}) fusion(f32[3,128,1024]{2,1,0:T(8,128)S(1)} %bitcast.48, f32[1024]{0:T(1024)S(1)} %bitcast.61, f32[1024]{0:T(1024)S(1)} %bitcast.63, f32[1024]{0:T(1024)S(1)} %bitcast.64, f32[1024]{0:T(1024)S(1)} %bitcast.65, f32[1024]{0:T(1024)S(1)} %bitcast.66, ...), kind=kLoop, calls=%fused_computation.120 | loop fusion | flops 25165056 | bytes 3275776 | tf_op jit(solution)/shard_map/reduce_sum | solution.py:52
  182.2 2.5 all-reduce.1
  184.7 0.6 multiply_convert_fusion.1
  185.2 59.1 %all-gather.14.cloned.1.call-done = bf16[2048,1024]{1,0:T(8,128)(2,1)} async-done(((bf16[256,1024]{1,0:T(8,128)(2,1)}), bf16[2048,1024]{1,0:T(8,128)(2,1)}) %all-gather.14.cloned.1.call-update) | async-done | bytes 4194320 | tf_op jit(solution)/shard_map/all_gather | solution.py:60
  244.4 5.2 convolution_convert_fusion
  249.6 0.0 all-gather.16.cloned.1.call-start
  249.7 7.6 %reduce-scatter.3.cloned.1.call-done = bf16[384,1024]{1,0:T(8,128)(2,1)} async-done(((bf16[384,2048]{1,0:T(8,128)(2,1)}), bf16[384,1024]{1,0:T(8,128)(2,1)}) %reduce-scatter.3.cloned.1.call-update) | async-done | bytes 786448 | tf_op jit(solution)/shard_map/reduce_scatter | solution.py:61
  257.3 2.3 add_convert_fusion.1
  259.6 0.0 all-gather.18.cloned.1.call-start
  259.6 0.7 all-gather.18.cloned.1.call-update
  260.4 0.7 all-gather.20.cloned.1.call-update
  261.1 0.2 reduce-scatter.5.cloned.1.call-start
  261.3 9.5 %all-gather.16.cloned.1.call-done = bf16[384,2048]{1,0:T(8,128)(2,1)} async-done(((bf16[384,1024]{1,0:T(8,128)(2,1)}), bf16[384,2048]{1,0:T(8,128)(2,1)}) %all-gather.16.cloned.1.call-update) | async-done | bytes 1572880 | tf_op jit(solution)/shard_map/all_gather | solution.py:65
  270.8 1.9 fusion.3
  272.8 177.6 %all-gather.18.cloned.1.call-done = bf16[2048,3072]{1,0:T(8,128)(2,1)} async-done(((bf16[256,3072]{1,0:T(8,128)(2,1)}), bf16[2048,3072]{1,0:T(8,128)(2,1)}) %all-gather.18.cloned.1.call-update) | async-done | bytes 12582928 | tf_op jit(solution)/shard_map/all_gather | solution.py:69
  450.3 176.5 %all-gather.20.cloned.1.call-done = bf16[2048,3072]{1,0:T(8,128)(2,1)} async-done(((bf16[256,3072]{1,0:T(8,128)(2,1)}), bf16[2048,3072]{1,0:T(8,128)(2,1)}) %all-gather.20.cloned.1.call-update) | async-done | bytes 12582928 | tf_op jit(solution)/shard_map/all_gather | solution.py:72
  626.8 15.3 %convolution_convert_fusion.1 = bf16[384,2048]{1,0:T(8,128)(2,1)} fusion(bf16[2048,3072]{1,0:T(8,128)(2,1)} %all-gather.20.cloned.1.call-done, bf16[2048,3072]{1,0:T(8,128)(2,1)} %all-gather.18.cloned.1.call-done, bf16[384,2048]{1,0:T(8,128)(2,1)S(1)} %copy-done.3, f32[2048]{0:T(1024)S(1)} %copy-done.5, f32[384]{0:T(512)S(1)} %add_rsqrt_fusion), kind=kOutput, calls=%fused_computation.42 | convolution fusion | flops 9671147520 | bytes 28321280 | tf_op jit(solution)/shard_map/dot_general | solution.py:19
  642.2 7.3 %reduce-scatter.5.cloned.1.call-done = bf16[384,1024]{1,0:T(8,128)(2,1)} async-done(((bf16[384,2048]{1,0:T(8,128)(2,1)}), bf16[384,1024]{1,0:T(8,128)(2,1)}) %reduce-scatter.5.cloned.1.call-update) | async-done | bytes 786448 | tf_op jit(solution)/shard_map/reduce_scatter | solution.py:73
  649.5 2.3 add_convert_fusion
  (25 shorter events, 0.3 us)
Async XLA Ops:
  6.5 14.9 %all-gather.8.cloned.1.call-start = ((), (), s32[]{:S(2)}) async-start(), calls=%async_computation.2 | async-start | bytes 2359296 | tf_op jit(solution)/shard_map/all_gather | solution.py:30
  7.3 90.3 %all-gather.12.cloned.1.call-start = ((), (), s32[]{:S(2)}) async-start(), calls=%async_computation.4 | async-start | bytes 4718592 | tf_op jit(solution)/shard_map/all_gather | solution.py:40
  8.0 89.6 %copy-start.4 = (f32[2048]{0:T(1024)S(1)}, f32[2048]{0:T(1024)}, u32[]{:S(2)}) copy-start(f32[2048]{0:T(1024)} %param.11) | copy-start | bytes 24580
  8.0 163.0 %all-gather.10.cloned.1.call-start = ((), (), s32[]{:S(2)}) async-start(), calls=%async_computation.3 | async-start | bytes 4718592 | tf_op jit(solution)/shard_map/all_gather | solution.py:35
  8.8 235.6 %all-gather.14.cloned.1.call-start = ((), (), s32[]{:S(2)}) async-start(), calls=%async_computation.5 | async-start | bytes 4718592 | tf_op jit(solution)/shard_map/all_gather | solution.py:60
  9.3 247.9 %reduce-scatter.3.cloned.1.call-start = ((), (), s32[]{:S(2)}) async-start(), calls=%async_computation.6 | async-start | bytes 2359296 | tf_op jit(solution)/shard_map/reduce_scatter | solution.py:61
  21.4 76.1 %copy-start.2 = (bf16[384,2048]{1,0:T(8,128)(2,1)S(1)}, bf16[384,2048]{1,0:T(8,128)(2,1)}, u32[]{:S(2)}) copy-start(bf16[384,2048]{1,0:T(8,128)(2,1)} %all-gather.8.cloned.1.call-done) | copy-start | bytes 4718596
  175.2 9.5 %dynamic-slice-start = ((f32[2048]{0:T(1024)}, s32[]{:T(128)}), f32[1024]{0:T(1024)S(1)}, s32[]{:S(2)}) async-start(f32[2048]{0:T(1024)} %param.15, s32[]{:T(128)} %select_n.4), calls=%async_computation.11 | async-start | bytes 8704 | tf_op jit(solution)/shard_map/dynamic_slice | solution.py:56
  249.6 7.7 %copy-start.1 = (bf16[384,1024]{1,0:T(8,128)(2,1)S(1)}, bf16[384,1024]{1,0:T(8,128)(2,1)}, u32[]{:S(2)}) copy-start(bf16[384,1024]{1,0:T(8,128)(2,1)} %param.10) | copy-start | bytes 2359300
  249.6 21.2 %all-gather.16.cloned.1.call-start = ((), (), s32[]{:S(2)}) async-start(), calls=%async_computation.7 | async-start | bytes 2359296 | tf_op jit(solution)/shard_map/all_gather | solution.py:65
  259.6 190.7 %all-gather.18.cloned.1.call-start = ((), (), s32[]{:S(2)}) async-start(), calls=%async_computation.8 | async-start | bytes 14155776 | tf_op jit(solution)/shard_map/all_gather | solution.py:69
  260.3 366.5 %copy-start.5 = (f32[2048]{0:T(1024)S(1)}, f32[2048]{0:T(1024)}, u32[]{:S(2)}) copy-start(f32[2048]{0:T(1024)} %param.17) | copy-start | bytes 24580
  260.4 366.5 %all-gather.20.cloned.1.call-start = ((), (), s32[]{:S(2)}) async-start(), calls=%async_computation.9 | async-start | bytes 14155776 | tf_op jit(solution)/shard_map/all_gather | solution.py:72
  261.1 388.4 %reduce-scatter.5.cloned.1.call-start = ((), (), s32[]{:S(2)}) async-start(), calls=%async_computation.10 | async-start | bytes 2359296 | tf_op jit(solution)/shard_map/reduce_scatter | solution.py:73
  270.8 356.0 %copy-start.3 = (bf16[384,2048]{1,0:T(8,128)(2,1)S(1)}, bf16[384,2048]{1,0:T(8,128)(2,1)}, u32[]{:S(2)}) copy-start(bf16[384,2048]{1,0:T(8,128)(2,1)} %all-gather.16.cloned.1.call-done) | copy-start | bytes 4718596
  642.2 7.3 %copy-start = (bf16[384,1024]{1,0:T(8,128)(2,1)S(1)}, bf16[384,1024]{1,0:T(8,128)(2,1)}, u32[]{:S(2)}) copy-start(bf16[384,1024]{1,0:T(8,128)(2,1)} %add_convert_fusion.1) | copy-start | bytes 2359300
Sparse Core Ops, SparseCore 0:
  8.9 12.5 all-gather.7
  23.6 73.9 all-gather.11
  99.7 71.3 all-gather.9
  173.0 71.3 all-gather.13
  249.7 7.4 reduce-scatter.2
  259.7 11.0 all-gather.15
  273.0 177.2 all-gather.17
  452.5 174.2 all-gather.19
  642.3 7.1 reduce-scatter.4
where the time goes:
time: 659 us; the launch traced here: 658 us
  waiting for transfers between devices  594 us (90%)
  matrix products  28.7 us (4%)
  other arithmetic  16.1 us (2%)
  between operations  13.3 us (2%)
    all_gather x1, waiting for transfers between devices, body(): lax.all_gather(w_up, 'fs', axis=0, tiled=True)  178 us
    all_gather x1, waiting for transfers between devices, body(): lax.all_gather(w_down_t, 'fs', axis=0, tiled=True)  176 us
    all_gather x1, waiting for transfers between devices, body(): lax.all_gather(w_gate, 'fs', axis=0, tiled=True)  74.2 us
    all_gather x1, waiting for transfers between devices, body(): lax.all_gather(w_value, 'fs', axis=0, tiled=True)  69.5 us
    all_gather x1, waiting for transfers between devices, body(): lax.all_gather(w_mix_out, 'fs', axis=0, tiled=True)  59.1 us
    dot_general x2, matrix products, times_transposed(): lax.dot_general(left, right, (((1,), (1,)), ((), ())), preferred_element_...  20.6 us
  transfers between devices with their start and end apart: 9, of which 9 were waited for; matrix products, arithmetic and copies ran while one was open for 3% of the time, Pallas kernels for 0%

commit v1 on v0

--- a/solution.py
+++ b/solution.py
@@ -1,3 +1,4 @@
+import functools
 import jax
 import jax.numpy as jnp
 from jax import lax
@@ -7,6 +8,49 @@
 KWIDTH = 31
 LENGTH = 128
 EPS = 1e-06
+
+
+def place_copies(m, device_axis, axis_no):
+    current_arr, item_now, back = (
+        lax.psum(1, device_axis),
+        lax.axis_index(device_axis),
+        m.shape[axis_no],
+    )
+    current_value = lax.dynamic_update_slice_in_dim(
+        jnp.zeros(
+            [
+                hop_no * current_arr if num == axis_no else hop_no
+                for num, hop_no in enumerate(m.shape)
+            ],
+            m.dtype,
+        ),
+        m,
+        item_now * back,
+        axis=axis_no,
+    )
+    seen_now = q_next = m
+    for i0 in range(1, current_arr // 2 + 1):
+        seen_now = lax.ppermute(
+            seen_now,
+            device_axis,
+            perm=[(num, (num + 1) % current_arr) for num in range(current_arr)],
+        )
+        current_value = lax.dynamic_update_slice_in_dim(
+            current_value, seen_now, (item_now - i0) % current_arr * back, axis=axis_no
+        )
+        if 2 * i0 < current_arr:
+            q_next = lax.ppermute(
+                q_next,
+                device_axis,
+                perm=[(num, (num - 1) % current_arr) for num in range(current_arr)],
+            )
+            current_value = lax.dynamic_update_slice_in_dim(
+                current_value, q_next, (item_now + i0) % current_arr * back, axis=axis_no
+            )
+    return current_value
+
+
+shards_time = functools.partial(place_copies, device_axis="fs", axis_no=0)
 
 
 def rms_norm(rows, gain):
@@ -30,11 +74,7 @@
     whole_rows = lax.all_gather(states, "tp", axis=1, tiled=True)
     normed = rms_norm(whole_rows, mix_gain)
     columns = normed
-    value = jnp.dot(
-        columns,
-        lax.all_gather(w_value, "fs", axis=0, tiled=True),
-        preferred_element_type=jnp.float32,
-    )
+    value = jnp.dot(columns, shards_time(w_value), preferred_element_type=jnp.float32)
     gate = jnp.dot(
         columns,
         lax.all_gather(w_gate, "fs", axis=0, tiled=True),

time: 659 us -> 626 us (0.950)
  waiting for transfers between devices: 594 us -> 533 us
  starting transfers between devices: 0.49 us -> 19.4 us
  local copies, waits for them, and re-layouts: 2.87 us -> 12 us
    ppermute x0 -> x7, waiting for transfers between devices: none -> 77.8 us  [the longest x4 70.6 us: place_copies(): lax.ppermute(seen_now, device_axis, perm=[(num, (num + 1) % current_arr)...]
    all_gather x1 -> x0, waiting for transfers between devices: 69.5 us -> none  [body(): lax.all_gather(w_value, 'fs', axis=0, tiled=True)]
    all_gather x1, waiting for transfers between devices: 74.2 us -> 17.1 us  [body(): lax.all_gather(w_gate, 'fs', axis=0, tiled=True)]
    ppermute x0 -> x7, starting transfers between devices: none -> 19 us  [the longest x3 11 us: place_copies(): lax.ppermute(q_next, device_axis, perm=[(num, (num - 1) % current_arr) fo...]
    all_gather x1, waiting for transfers between devices: 9.21 us -> 0.01 us  [body(): whole_rows = lax.all_gather(states, 'tp', axis=1, tiled=True)]
    dynamic_update_slice x0 -> x8, local copies, waits for them, and re-layouts: none -> 6.74 us  [the longest x4 3.33 us: place_copies(): lax.dynamic_update_slice_in_dim(current_value, seen_now, (item_now - i0)...]
  transfers between devices with their start and end apart: 9 -> 15, of which waited for: 9 -> 12; matrix products, arithmetic and copies ran while one was open for 3% -> 5% of each run, Pallas kernels for 0% -> 0%
where the time goes in v1:
time: 626 us
  waiting for transfers between devices  533 us (85%)
  matrix products  28.6 us (5%)
  starting transfers between devices  19.4 us (3%)
  other arithmetic  16.1 us (3%)
  between operations  13.7 us (2%)
  local copies, waits for them, and re-layouts  12 us (2%)
    all_gather x1, waiting for transfers between devices, body(): lax.all_gather(w_up, 'fs', axis=0, tiled=True)  177 us
    all_gather x1, waiting for transfers between devices, body(): lax.all_gather(w_down_t, 'fs', axis=0, tiled=True)  176 us
    ppermute x4, waiting for transfers between devices, place_copies(): lax.ppermute(seen_now, device_axis, perm=[(num, (num + 1) % current_arr)...  70.6 us
    all_gather x1, waiting for transfers between devices, body(): lax.all_gather(w_mix_out, 'fs', axis=0, tiled=True)  56.5 us
    dot_general x2, matrix products, times_transposed(): lax.dot_general(left, right, (((1,), (1,)), ((), ())), preferred_element_...  20.5 us
    all_gather x1, waiting for transfers between devices, body(): lax.all_gather(w_gate, 'fs', axis=0, tiled=True)  17.1 us
  transfers between devices with their start and end apart: 15, of which 12 were waited for; matrix products, arithmetic and copies ran while one was open for 5% of the time, Pallas kernels for 0%

profile of v1, /device:TPU:0, one launch (start us, length us, event | category | flops | bytes accessed | tf_op | source)
XLA Modules:
  0.0 625.6 jit_solution(15937728451691553155)
XLA Ops:
  8.8 3.0 collective-permute-start
  11.8 3.1 collective-permute-start.1
  15.0 21.1 %collective-permute-done = bf16[256,1024]{1,0:T(8,128)(2,1)S(1)} collective-permute-done((bf16[256,1024]{1,0:T(8,128)(2,1)S(1)}, bf16[256,1024]{1,0:T(8,128)(2,1)S(1)}, u32[]{:S(2)}, u32[]{:S(2)}) %collective-permute-start) | collective-permute-done | bytes 524320 | tf_op jit(solution)/shard_map/ppermute | solution.py:33
  36.1 2.5 collective-permute-start.2
  38.5 3.1 collective-permute-start.3
  41.6 1.5 constant_dynamic-slice_fusion
  43.1 2.5 broadcast_in_dim.2
  45.6 0.9 constant_dynamic-update-slice_fusion.7
  46.5 17.9 %collective-permute-done.2 = bf16[256,1024]{1,0:T(8,128)(2,1)S(1)} collective-permute-done((bf16[256,1024]{1,0:T(8,128)(2,1)S(1)}, bf16[256,1024]{1,0:T(8,128)(2,1)S(1)}, u32[]{:S(2)}, u32[]{:S(2)}) %collective-permute-start.2) | collective-permute-done | bytes 524320 | tf_op jit(solution)/shard_map/ppermute | solution.py:33
  64.4 1.3 fusion.79
  65.8 4.8 collective-permute-start.5
  73.9 24.0 %collective-permute-done.4 = bf16[256,1024]{1,0:T(8,128)(2,1)S(1)} collective-permute-done((bf16[256,1024]{1,0:T(8,128)(2,1)S(1)}, bf16[256,1024]{1,0:T(8,128)(2,1)S(1)}, u32[]{:S(2)}, u32[]{:S(2)}) %collective-permute-start.4) | collective-permute-done | bytes 524320 | tf_op jit(solution)/shard_map/ppermute | solution.py:33
  97.9 2.5 collective-permute-start.6
  101.3 7.2 %collective-permute-done.5 = bf16[256,1024]{1,0:T(8,128)(2,1)S(1)} collective-permute-done((bf16[256,1024]{1,0:T(8,128)(2,1)S(1)}, bf16[256,1024]{1,0:T(8,128)(2,1)S(1)}, u32[]{:S(2)}, u32[]{:S(2)}) %collective-permute-start.5) | collective-permute-done | bytes 524320 | tf_op jit(solution)/shard_map/ppermute | solution.py:42
  109.4 1.9 fusion
  111.3 7.6 %collective-permute-done.6 = bf16[256,1024]{1,0:T(8,128)(2,1)S(1)} collective-permute-done((bf16[256,1024]{1,0:T(8,128)(2,1)S(1)}, bf16[256,1024]{1,0:T(8,128)(2,1)S(1)}, u32[]{:S(2)}, u32[]{:S(2)}) %collective-permute-start.6) | collective-permute-done | bytes 524320 | tf_op jit(solution)/shard_map/ppermute | solution.py:33
  119.7 17.1 %all-gather.9.cloned.1.call-done = bf16[2048,1024]{1,0:T(8,128)(2,1)} async-done(((bf16[256,1024]{1,0:T(8,128)(2,1)}), bf16[2048,1024]{1,0:T(8,128)(2,1)}) %all-gather.9.cloned.1.call-update) | async-done | bytes 4194320 | tf_op jit(solution)/shard_map/all_gather | solution.py:80
  136.8 4.0 fusion.73
  140.9 4.1 divide_multiply_fusion
  145.0 7.0 %fusion.77 = (f32[3,128]{1,0:T(4,128)S(1)}, f32[3,128]{1,0:T(4,128)S(1)}, f32[3,128,1024]{2,1,0:T(8,128)S(1)}) fusion(f32[3,128,1024]{2,1,0:T(8,128)S(1)} %bitcast.48, f32[1024]{0:T(1024)S(1)} %bitcast.61, f32[1024]{0:T(1024)S(1)} %bitcast.63, f32[1024]{0:T(1024)S(1)} %bitcast.64, f32[1024]{0:T(1024)S(1)} %bitcast.65, f32[1024]{0:T(1024)S(1)} %bitcast.66, ...), kind=kLoop, calls=%fused_computation.128 | loop fusion | flops 25165056 | bytes 3275776 | tf_op jit(solution)/shard_map/reduce_sum | solution.py:92
  152.0 2.5 all-reduce.1
  155.1 56.5 %all-gather.11.cloned.1.call-done = bf16[2048,1024]{1,0:T(8,128)(2,1)} async-done(((bf16[256,1024]{1,0:T(8,128)(2,1)}), bf16[2048,1024]{1,0:T(8,128)(2,1)}) %all-gather.11.cloned.1.call-update) | async-done | bytes 4194320 | tf_op jit(solution)/shard_map/all_gather | solution.py:100
  211.5 5.2 convolution_convert_fusion
  216.8 7.6 %reduce-scatter.3.cloned.1.call-done = bf16[384,1024]{1,0:T(8,128)(2,1)} async-done(((bf16[384,2048]{1,0:T(8,128)(2,1)}), bf16[384,1024]{1,0:T(8,128)(2,1)}) %reduce-scatter.3.cloned.1.call-update) | async-done | bytes 786448 | tf_op jit(solution)/shard_map/reduce_scatter | solution.py:101
  224.4 2.3 add_convert_fusion.1
  228.3 9.7 %all-gather.13.cloned.1.call-done = bf16[384,2048]{1,0:T(8,128)(2,1)} async-done(((bf16[384,1024]{1,0:T(8,128)(2,1)}), bf16[384,2048]{1,0:T(8,128)(2,1)}) %all-gather.13.cloned.1.call-update) | async-done | bytes 1572880 | tf_op jit(solution)/shard_map/all_gather | solution.py:105
  237.9 1.9 fusion.3
  239.9 177.4 %all-gather.15.cloned.1.call-done = bf16[2048,3072]{1,0:T(8,128)(2,1)} async-done(((bf16[256,3072]{1,0:T(8,128)(2,1)}), bf16[2048,3072]{1,0:T(8,128)(2,1)}) %all-gather.15.cloned.1.call-update) | async-done | bytes 12582928 | tf_op jit(solution)/shard_map/all_gather | solution.py:109
  417.3 176.5 %all-gather.17.cloned.1.call-done = bf16[2048,3072]{1,0:T(8,128)(2,1)} async-done(((bf16[256,3072]{1,0:T(8,128)(2,1)}), bf16[2048,3072]{1,0:T(8,128)(2,1)}) %all-gather.17.cloned.1.call-update) | async-done | bytes 12582928 | tf_op jit(solution)/shard_map/all_gather | solution.py:112
  593.8 15.3 %convolution_convert_fusion.1 = bf16[384,2048]{1,0:T(8,128)(2,1)} fusion(bf16[2048,3072]{1,0:T(8,128)(2,1)} %all-gather.17.cloned.1.call-done, bf16[2048,3072]{1,0:T(8,128)(2,1)} %all-gather.15.cloned.1.call-done, bf16[384,2048]{1,0:T(8,128)(2,1)S(1)} %copy-done.3, f32[2048]{0:T(1024)S(1)} %copy-done.6, f32[384]{0:T(512)S(1)} %add_rsqrt_fusion), kind=kOutput, calls=%fused_computation.42 | convolution fusion | flops 9671147520 | bytes 28321280 | tf_op jit(solution)/shard_map/dot_general | solution.py:63
  609.2 7.3 %reduce-scatter.5.cloned.1.call-done = bf16[384,1024]{1,0:T(8,128)(2,1)} async-done(((bf16[384,2048]{1,0:T(8,128)(2,1)}), bf16[384,1024]{1,0:T(8,128)(2,1)}) %reduce-scatter.5.cloned.1.call-update) | async-done | bytes 786448 | tf_op jit(solution)/shard_map/reduce_scatter | solution.py:113
  616.4 2.3 add_convert_fusion
  (47 shorter events, 10.3 us)
Async XLA Ops:
  6.5 2.3 copy-start.4
  6.5 102.8 %all-gather.7.cloned.1.call-start = ((), (), s32[]{:S(2)}) async-start(), calls=%async_computation.2 | async-start | bytes 2359296 | tf_op jit(solution)/shard_map/all_gather | solution.py:74
  7.3 129.6 %all-gather.9.cloned.1.call-start = ((), (), s32[]{:S(2)}) async-start(), calls=%async_computation.3 | async-start | bytes 4718592 | tf_op jit(solution)/shard_map/all_gather | solution.py:80
  8.0 203.5 %all-gather.11.cloned.1.call-start = ((), (), s32[]{:S(2)}) async-start(), calls=%async_computation.4 | async-start | bytes 4718592 | tf_op jit(solution)/shard_map/all_gather | solution.py:100
  8.7 215.6 %reduce-scatter.3.cloned.1.call-start = ((), (), s32[]{:S(2)}) async-start(), calls=%async_computation.5 | async-start | bytes 2359296 | tf_op jit(solution)/shard_map/reduce_scatter | solution.py:101
  8.8 27.3 %collective-permute-start = (bf16[256,1024]{1,0:T(8,128)(2,1)S(1)}, bf16[256,1024]{1,0:T(8,128)(2,1)S(1)}, u32[]{:S(2)}, u32[]{:S(2)}) collective-permute-start(bf16[256,1024]{1,0:T(8,128)(2,1)S(1)} %copy-done.4), channel_id=1, source_target_pairs={{0,2},{2,4},{4,6},{6,8},{8,10},{10,12},{12,14},{14,0},{1,3},{3,5},... | collective-permute-start | bytes 1572872 | tf_op jit(solution)/shard_map/ppermute | solution.py:33
  11.8 26.7 %collective-permute-start.1 = (bf16[256,1024]{1,0:T(8,128)(2,1)S(1)}, bf16[256,1024]{1,0:T(8,128)(2,1)S(1)}, u32[]{:S(2)}, u32[]{:S(2)}) collective-permute-start(bf16[256,1024]{1,0:T(8,128)(2,1)S(1)} %copy-done.4), channel_id=1, source_target_pairs={{0,14},{2,0},{4,2},{6,4},{8,6},{10,8},{12,10},{14,12},{1,15},{3,1}... | collective-permute-start | bytes 1572872 | tf_op jit(solution)/shard_map/ppermute | solution.py:42
  36.1 28.3 %collective-permute-start.2 = (bf16[256,1024]{1,0:T(8,128)(2,1)S(1)}, bf16[256,1024]{1,0:T(8,128)(2,1)S(1)}, u32[]{:S(2)}, u32[]{:S(2)}) collective-permute-start(bf16[256,1024]{1,0:T(8,128)(2,1)S(1)} %collective-permute-done), channel_id=1, source_target_pairs={{0,2},{2,4},{4,6},{6,8},{8,10},{10,12},{12,14},{14,0},{1,3},{3,5},... | collective-permute-start | bytes 1572872 | tf_op jit(solution)/shard_map/ppermute | solution.py:33
  38.5 27.3 %collective-permute-start.3 = (bf16[256,1024]{1,0:T(8,128)(2,1)S(1)}, bf16[256,1024]{1,0:T(8,128)(2,1)S(1)}, u32[]{:S(2)}, u32[]{:S(2)}) collective-permute-start(bf16[256,1024]{1,0:T(8,128)(2,1)S(1)} %collective-permute-done.1), channel_id=1, source_target_pairs={{0,14},{2,0},{4,2},{6,4},{8,6},{10,8},{12,10},{14,12},{1,15},{3,1}... | collective-permute-start | bytes 1572872 | tf_op jit(solution)/shard_map/ppermute | solution.py:42
  64.4 33.5 %collective-permute-start.4 = (bf16[256,1024]{1,0:T(8,128)(2,1)S(1)}, bf16[256,1024]{1,0:T(8,128)(2,1)S(1)}, u32[]{:S(2)}, u32[]{:S(2)}) collective-permute-start(bf16[256,1024]{1,0:T(8,128)(2,1)S(1)} %collective-permute-done.2), channel_id=1, source_target_pairs={{0,2},{2,4},{4,6},{6,8},{8,10},{10,12},{12,14},{14,0},{1,3},{3,5},... | collective-permute-start | bytes 1572872 | tf_op jit(solution)/shard_map/ppermute | solution.py:33
  65.8 42.7 %collective-permute-start.5 = (bf16[256,1024]{1,0:T(8,128)(2,1)S(1)}, bf16[256,1024]{1,0:T(8,128)(2,1)S(1)}, u32[]{:S(2)}, u32[]{:S(2)}) collective-permute-start(bf16[256,1024]{1,0:T(8,128)(2,1)S(1)} %collective-permute-done.3), channel_id=1, source_target_pairs={{0,14},{2,0},{4,2},{6,4},{8,6},{10,8},{12,10},{14,12},{1,15},{3,1}... | collective-permute-start | bytes 1572872 | tf_op jit(solution)/shard_map/ppermute | solution.py:42
  97.9 20.9 %collective-permute-start.6 = (bf16[256,1024]{1,0:T(8,128)(2,1)S(1)}, bf16[256,1024]{1,0:T(8,128)(2,1)S(1)}, u32[]{:S(2)}, u32[]{:S(2)}) collective-permute-start(bf16[256,1024]{1,0:T(8,128)(2,1)S(1)} %collective-permute-done.4), channel_id=1, source_target_pairs={{0,2},{2,4},{4,6},{6,8},{8,10},{10,12},{12,14},{14,0},{1,3},{3,5},... | collective-permute-start | bytes 1572872 | tf_op jit(solution)/shard_map/ppermute | solution.py:33
  109.4 27.5 %copy-start.5 = (f32[2048]{0:T(1024)S(1)}, f32[2048]{0:T(1024)}, u32[]{:S(2)}) copy-start(f32[2048]{0:T(1024)} %param.11) | copy-start | bytes 24580
  109.4 27.5 %copy-start.2 = (bf16[384,2048]{1,0:T(8,128)(2,1)S(1)}, bf16[384,2048]{1,0:T(8,128)(2,1)}, u32[]{:S(2)}) copy-start(bf16[384,2048]{1,0:T(8,128)(2,1)} %all-gather.7.cloned.1.call-done) | copy-start | bytes 4718596
  145.0 9.5 %dynamic-slice-start = ((f32[2048]{0:T(1024)}, s32[]{:T(128)}), f32[1024]{0:T(1024)S(1)}, s32[]{:S(2)}) async-start(f32[2048]{0:T(1024)} %param.15, s32[]{:T(128)} %select_n.59), calls=%async_computation.10 | async-start | bytes 8704 | tf_op jit(solution)/shard_map/dynamic_slice | solution.py:96
  216.7 7.7 %copy-start.1 = (bf16[384,1024]{1,0:T(8,128)(2,1)S(1)}, bf16[384,1024]{1,0:T(8,128)(2,1)}, u32[]{:S(2)}) copy-start(bf16[384,1024]{1,0:T(8,128)(2,1)} %param.10) | copy-start | bytes 2359300
  216.7 21.2 %all-gather.13.cloned.1.call-start = ((), (), s32[]{:S(2)}) async-start(), calls=%async_computation.6 | async-start | bytes 2359296 | tf_op jit(solution)/shard_map/all_gather | solution.py:105
  226.7 190.6 %all-gather.15.cloned.1.call-start = ((), (), s32[]{:S(2)}) async-start(), calls=%async_computation.7 | async-start | bytes 14155776 | tf_op jit(solution)/shard_map/all_gather | solution.py:109
  227.3 366.5 %copy-start.6 = (f32[2048]{0:T(1024)S(1)}, f32[2048]{0:T(1024)}, u32[]{:S(2)}) copy-start(f32[2048]{0:T(1024)} %param.17) | copy-start | bytes 24580
  227.3 366.5 %all-gather.17.cloned.1.call-start = ((), (), s32[]{:S(2)}) async-start(), calls=%async_computation.8 | async-start | bytes 14155776 | tf_op jit(solution)/shard_map/all_gather | solution.py:112
  228.0 388.4 %reduce-scatter.5.cloned.1.call-start = ((), (), s32[]{:S(2)}) async-start(), calls=%async_computation.9 | async-start | bytes 2359296 | tf_op jit(solution)/shard_map/reduce_scatter | solution.py:113
  237.9 355.9 %copy-start.3 = (bf16[384,2048]{1,0:T(8,128)(2,1)S(1)}, bf16[384,2048]{1,0:T(8,128)(2,1)}, u32[]{:S(2)}) copy-start(bf16[384,2048]{1,0:T(8,128)(2,1)} %all-gather.13.cloned.1.call-done) | copy-start | bytes 4718596
  609.1 7.3 %copy-start = (bf16[384,1024]{1,0:T(8,128)(2,1)S(1)}, bf16[384,1024]{1,0:T(8,128)(2,1)}, u32[]{:S(2)}) copy-start(bf16[384,1024]{1,0:T(8,128)(2,1)} %add_convert_fusion.1) | copy-start | bytes 2359300
Sparse Core Ops, SparseCore 0:
  8.9 12.5 all-gather.6
  23.6 113.2 all-gather.8
  139.0 72.5 all-gather.10
  216.9 7.4 reduce-scatter.2
  226.8 11.0 all-gather.12
  240.0 177.2 all-gather.14
  419.5 174.2 all-gather.16
  609.3 7.0 reduce-scatter.4
